TPU v7x, 32 devices: a whole 2x2x4 slice. The times are simulated.
32 devices in a mesh: rep: 2 (over y), fs: 4 (over z), tp: 4 (over x, core).
Axes of the slice: x: 2, y: 2, z: 4, core: 2. Of those that a mesh axis runs over, the one named last changes fastest.
Arguments:
- stream: bfloat16 [4096, 2048], P(('rep', 'fs', 'tp')), may hold values from -6 to 6
- gain_before: float32 [2048], replicated, may hold values from 0.1 to 1.9
- gain_after: float32 [2048], replicated, may hold values from 0.1 to 1.9
- proj_gate: bfloat16 [2048, 3584], P('fs', 'tp'), may hold values from -0.125 to 0.125
- proj_lift: bfloat16 [2048, 3584], P('fs', 'tp'), may hold values from -0.125 to 0.125
- proj_down: bfloat16 [3584, 2048], P('tp', 'fs'), may hold values from -0.09375 to 0.09375
- mixer_gain: float32 [2048], replicated, may hold values from 0.1 to 1.9
- mixer_u: bfloat16 [2048, 2048], P('fs', 'tp'), may hold values from -0.125 to 0.125
- mixer_v: bfloat16 [2048, 2048], P('fs', 'tp'), may hold values from -1 to 1
- layer_gain: float32 [2048], P('tp'), may hold values from 0.1 to 1.9
- layer_shift: float32 [2048], P('tp'), may hold values from -3 to 3
- spatial: bfloat16 [16, 128, 128], P('tp'), may hold values from -0.5 to 0.5
- spatial_shift: float32 [16, 128], P('tp'), may hold values from 0.2 to 2
- mixer_down: bfloat16 [2048, 2048], P('tp', 'fs'), may hold values from -0.125 to 0.125
Outputs:
- result: bfloat16 [4096, 2048], P(('rep', 'fs', 'tp'))
All inputs are finite; a program needn't handle non-finite values.
Results may differ from a plain program's by a relative error of at most 0.017.
Values may be sent and summed in bfloat16 or wider, within the bound.
A program may use at most 128 MiB of HBM per device.

v0:
```python
import jax
import jax.numpy as jnp
from jax import lax
from jax.sharding import PartitionSpec as P

GROUP_DIM = 128
SPAN = 128
A = 2048
norm_epsilon = 1e-06
layer_epsilon = 1e-05


def norm_rows(row_block, scale_gain):
    widened = row_block.astype(jnp.float32)
    factor = lax.rsqrt(jnp.mean(widened * widened, axis=1, keepdims=True) + norm_epsilon)
    return (widened * factor * scale_gain).astype(jnp.bfloat16)


def gathered_norm(stream_rows, scale_gain):
    gathered = lax.all_gather(stream_rows, "tp", axis=0, tiled=True)
    return norm_rows(gathered, scale_gain)


def pair_adder(normed, pieces):
    return (
        jnp.dot(normed, pieces[0], preferred_element_type=jnp.float32),
        jnp.dot(normed, pieces[1], preferred_element_type=jnp.float32),
    )


def activate(gate_vals, lift_vals):
    return (jax.nn.silu(gate_vals) * lift_vals).astype(jnp.bfloat16)


def half_again(stream_rows, scale_gain, proj_gate, proj_lift, proj_down):
    normed = gathered_norm(stream_rows, scale_gain)
    gate_vals, lift_vals = pair_adder(
        normed,
        (
            lax.all_gather(proj_gate, "fs", axis=0, tiled=True),
            lax.all_gather(proj_lift, "fs", axis=0, tiled=True),
        ),
    )
    hidden = activate(gate_vals, lift_vals)
    partial_value = jnp.dot(
        hidden,
        lax.all_gather(proj_down, "fs", axis=1, tiled=True),
        preferred_element_type=jnp.float32,
    )
    summed = lax.psum_scatter(
        partial_value.astype(jnp.bfloat16), "tp", scatter_dimension=0, tiled=True
    ).astype(jnp.float32)
    return (stream_rows.astype(jnp.float32) + 0.5 * summed).astype(jnp.bfloat16)


def token_mixer(
    stream_rows,
    mixer_gain,
    mixer_u,
    mixer_v,
    layer_gain,
    layer_shift,
    spatial,
    spatial_shift,
    mixer_down,
):
    gathered = lax.all_gather(stream_rows, "tp", axis=0, tiled=True)
    normed = norm_rows(gathered, mixer_gain)
    seq_tokens = normed.shape[0]
    u_vals, v_vals = pair_adder(
        normed,
        (
            lax.all_gather(mixer_u, "fs", axis=0, tiled=True),
            lax.all_gather(mixer_v, "fs", axis=0, tiled=True),
        ),
    )
    lifted = jax.nn.gelu(v_vals)
    moments = lax.psum((jnp.sum(lifted, axis=1), jnp.sum(lifted * lifted, axis=1)), "tp")
    centre = moments[0] / A
    spread = moments[1] / A - centre * centre
    normed_v = (
        (lifted - centre[:, None]) * lax.rsqrt(spread[:, None] + layer_epsilon) * layer_gain
        + layer_shift
    ).astype(jnp.bfloat16)
    groups_here = spatial.shape[0]
    blocked = normed_v.reshape(seq_tokens // SPAN, SPAN, groups_here, GROUP_DIM)
    causal = jnp.tril(jnp.ones((SPAN, SPAN), dtype=bool))
    masked = jnp.where(causal[None], spatial, jnp.zeros((), jnp.bfloat16))
    mixed_v = jnp.einsum("gts,bsgd->btgd", masked, blocked, preferred_element_type=jnp.float32)
    mixed_v = mixed_v + spatial_shift.T[None, :, :, None]
    gated = (jax.nn.gelu(u_vals) * mixed_v.reshape(seq_tokens, groups_here * GROUP_DIM)).astype(
        jnp.bfloat16
    )
    partial_value = jnp.dot(
        gated,
        lax.all_gather(mixer_down, "fs", axis=1, tiled=True),
        preferred_element_type=jnp.float32,
    )
    summed = lax.psum_scatter(
        partial_value.astype(jnp.bfloat16), "tp", scatter_dimension=0, tiled=True
    ).astype(jnp.float32)
    return (stream_rows.astype(jnp.float32) + summed).astype(jnp.bfloat16)


def body(
    stream,
    gain_before,
    gain_after,
    proj_gate,
    proj_lift,
    proj_down,
    mixer_gain,
    mixer_u,
    mixer_v,
    layer_gain,
    layer_shift,
    spatial,
    spatial_shift,
    mixer_down,
):
    first = half_again(stream, gain_before, proj_gate, proj_lift, proj_down)
    second = token_mixer(
        first,
        mixer_gain,
        mixer_u,
        mixer_v,
        layer_gain,
        layer_shift,
        spatial,
        spatial_shift,
        mixer_down,
    )
    result = half_again(second, gain_after, proj_gate, proj_lift, proj_down)
    return result


def solution(mesh):
    placed = (
        P(("rep", "fs", "tp"), None),
        P(),
        P(),
        P("fs", "tp"),
        P("fs", "tp"),
        P("tp", "fs"),
        P(),
        P("fs", "tp"),
        P("fs", "tp"),
        P("tp"),
        P("tp"),
        P("tp", None, None),
        P("tp", None),
        P("tp", "fs"),
    )
    return jax.shard_map(
        body, mesh=mesh, in_specs=placed, out_specs=P(("rep", "fs", "tp"), None), check_vma=False
    )
```

profile of v0, /device:TPU:0, one launch (start us, length us, event | category | flops | bytes accessed | tf_op | source)
XLA Modules:
  0.0 575.2 jit_solution(15976335767558670113)
XLA Ops:
  6.5 0.7 all-gather.10.cloned.1.call-update
  7.3 0.7 all-gather.12.cloned.1.call-update
  9.4 24.8 %all-gather.10.cloned.1.call-done = bf16[512,2048]{1,0:T(8,128)(2,1)} async-done(((bf16[128,2048]{1,0:T(8,128)(2,1)}), bf16[512,2048]{1,0:T(8,128)(2,1)}) %all-gather.10.cloned.1.call-update) | async-done | bytes 2097168 | tf_op jit(solution)/shard_map/all_gather | solution.py:20
  34.2 2.2 fusion
  36.4 71.5 %all-gather.12.cloned.1.call-done = bf16[2048,896]{1,0:T(8,128)(2,1)} async-done(((bf16[512,896]{1,0:T(8,128)(2,1)}), bf16[2048,896]{1,0:T(8,128)(2,1)}) %all-gather.12.cloned.1.call-update) | async-done | bytes 3670032 | tf_op jit(solution)/shard_map/all_gather | solution.py:40
  107.9 5.6 fusion.42
  113.5 66.6 %all-gather.14.cloned.1.call-done = bf16[2048,896]{1,0:T(8,128)(2,1)} async-done(((bf16[512,896]{1,0:T(8,128)(2,1)}), bf16[2048,896]{1,0:T(8,128)(2,1)}) %all-gather.14.cloned.1.call-update) | async-done | bytes 3670032 | tf_op jit(solution)/shard_map/all_gather | solution.py:41
  180.2 72.1 %all-gather.16.cloned.1.call-done = bf16[896,2048]{1,0:T(8,128)(2,1)} async-done(((bf16[896,512]{1,0:T(8,128)(2,1)}), bf16[896,2048]{1,0:T(8,128)(2,1)}) %all-gather.16.cloned.1.call-update) | async-done | bytes 3670032 | tf_op jit(solution)/shard_map/all_gather | solution.py:47
  252.3 9.7 %convolution_convert_fusion.1 = bf16[512,2048]{1,0:T(8,128)(2,1)} fusion(bf16[896,2048]{1,0:T(8,128)(2,1)} %all-gather.16.cloned.1.call-done, f32[512,896]{1,0:T(8,128)} %fusion.42, bf16[2048,896]{1,0:T(8,128)(2,1)} %all-gather.14.cloned.1.call-done, bf16[512,2048]{1,0:T(8,128)(2,1)S(1)} %copy-done.4, f32[2048]{0:T(1024)S(1)} %copy-done.10, ...), kind=kOutput, calls=%fused_computation.16 | convolution fusion | flops 3766091776 | bytes 13379584 | tf_op jit(solution)/shard_map/dot_general | solution.py:45
  262.0 29.9 %reduce-scatter.4.cloned.1.call-done = bf16[128,2048]{1,0:T(8,128)(2,1)} async-done(((bf16[512,2048]{1,0:T(8,128)(2,1)}), bf16[128,2048]{1,0:T(8,128)(2,1)}) %reduce-scatter.4.cloned.1.call-update) | async-done | bytes 524304 | tf_op jit(solution)/shard_map/reduce_scatter | solution.py:50
  291.9 2.0 add_convert_fusion.3
  294.0 0.7 all-gather.22.cloned.1.call-update
  296.2 20.4 %all-gather.18.cloned.1.call-done = bf16[512,2048]{1,0:T(8,128)(2,1)} async-done(((bf16[128,2048]{1,0:T(8,128)(2,1)}), bf16[512,2048]{1,0:T(8,128)(2,1)}) %all-gather.18.cloned.1.call-update) | async-done | bytes 2097168 | tf_op jit(solution)/shard_map/all_gather | solution.py:67
  316.6 2.2 fusion.3
  318.9 45.0 %all-gather.22.cloned.1.call-done = bf16[2048,512]{1,0:T(8,128)(2,1)} async-done(((bf16[512,512]{1,0:T(8,128)(2,1)}), bf16[2048,512]{1,0:T(8,128)(2,1)}) %all-gather.22.cloned.1.call-update) | async-done | bytes 2097168 | tf_op jit(solution)/shard_map/all_gather | solution.py:74
  363.9 4.1 fusion.60
  368.0 6.5 %all-reduce = (f32[512]{0:T(512)S(1)}, f32[512]{0:T(512)S(1)}) all-reduce(f32[512]{0:T(512)S(1)} %get-tuple-element.6, f32[512]{0:T(512)S(1)} %get-tuple-element.5), channel_id=1, replica_groups=mesh['rep'=2,'fs'=4,'tp'=4] {'tp'}, use_global_device_ids=true, to_apply=%region_6.7 | all-reduce | flops 1024 | bytes 8192 | tf_op jit(solution)/shard_map/psum | solution.py:78
  374.6 1.5 add_convert_fusion.2
  376.0 0.9 reshape.47
  377.0 1.4 fusion.9
  378.4 1.3 copy.21
  379.7 30.2 %all-gather.20.cloned.1.call-done = bf16[2048,512]{1,0:T(8,128)(2,1)} async-done(((bf16[512,512]{1,0:T(8,128)(2,1)}), bf16[2048,512]{1,0:T(8,128)(2,1)}) %all-gather.20.cloned.1.call-update) | async-done | bytes 2097168 | tf_op jit(solution)/shard_map/all_gather | solution.py:73
  409.9 46.1 %all-gather.24.cloned.1.call-done = bf16[512,2048]{1,0:T(8,128)(2,1)} async-done(((bf16[512,512]{1,0:T(8,128)(2,1)}), bf16[512,2048]{1,0:T(8,128)(2,1)}) %all-gather.24.cloned.1.call-update) | async-done | bytes 2097168 | tf_op jit(solution)/shard_map/all_gather | solution.py:96
  456.0 6.5 %convolution_convert_fusion.2 = bf16[512,2048]{1,0:T(8,128)(2,1)} fusion(bf16[512,2048]{1,0:T(8,128)(2,1)} %all-gather.24.cloned.1.call-done, f32[64,8,4,128]{3,2,1,0:T(4,128)} %bitcast.25, bf16[2048,512]{1,0:T(8,128)(2,1)} %all-gather.20.cloned.1.call-done, bf16[512,2048]{1,0:T(8,128)(2,1)S(1)} %copy-done.3, f32[2048]{0:T(1024)S(1)} %copy-done.11, ...), kind=kOutput, calls=%fused_computation.17 | convolution fusion | flops 2155347968 | bytes 9447424 | tf_op jit(solution)/shard_map/dot_general | solution.py:94
  462.6 30.1 %reduce-scatter.6.cloned.1.call-done = bf16[128,2048]{1,0:T(8,128)(2,1)} async-done(((bf16[512,2048]{1,0:T(8,128)(2,1)}), bf16[128,2048]{1,0:T(8,128)(2,1)}) %reduce-scatter.6.cloned.1.call-update) | async-done | bytes 524304 | tf_op jit(solution)/shard_map/reduce_scatter | solution.py:99
  492.7 2.0 add_convert_fusion.1
  494.9 22.5 %all-gather.26.cloned.1.call-done = bf16[512,2048]{1,0:T(8,128)(2,1)} async-done(((bf16[128,2048]{1,0:T(8,128)(2,1)}), bf16[512,2048]{1,0:T(8,128)(2,1)}) %all-gather.26.cloned.1.call-update) | async-done | bytes 2097168 | tf_op jit(solution)/shard_map/all_gather | solution.py:20
  517.4 2.2 fusion.6
  519.6 5.7 fusion.28
  525.3 9.7 %convolution_convert_fusion = bf16[512,2048]{1,0:T(8,128)(2,1)} fusion(bf16[896,2048]{1,0:T(8,128)(2,1)} %all-gather.16.cloned.1.call-done, f32[512,896]{1,0:T(8,128)} %fusion.28, bf16[2048,896]{1,0:T(8,128)(2,1)} %all-gather.14.cloned.1.call-done, bf16[512,2048]{1,0:T(8,128)(2,1)S(1)} %copy-done.5, f32[2048]{0:T(1024)S(1)} %copy-done.12, ...), kind=kOutput, calls=%fused_computation.15 | convolution fusion | flops 3766091776 | bytes 13379584 | tf_op jit(solution)/shard_map/dot_general | solution.py:45
  535.0 31.3 %reduce-scatter.8.cloned.1.call-done = bf16[128,2048]{1,0:T(8,128)(2,1)} async-done(((bf16[512,2048]{1,0:T(8,128)(2,1)}), bf16[128,2048]{1,0:T(8,128)(2,1)}) %reduce-scatter.8.cloned.1.call-update) | async-done | bytes 524304 | tf_op jit(solution)/shard_map/reduce_scatter | solution.py:50
  566.4 2.0 add_convert_fusion
  (52 shorter events, 3.4 us)
Async XLA Ops:
  6.5 27.7 %all-gather.10.cloned.1.call-start = ((), (), s32[]{:S(2)}) async-start(), calls=%async_computation.3 | async-start | bytes 2621440 | tf_op jit(solution)/shard_map/all_gather | solution.py:20
  7.3 100.6 %all-gather.12.cloned.1.call-start = ((), (), s32[]{:S(2)}) async-start(), calls=%async_computation.4 | async-start | bytes 4587520 | tf_op jit(solution)/shard_map/all_gather | solution.py:40
  8.0 99.9 %copy-start.10 = (f32[2048]{0:T(1024)S(1)}, f32[2048]{0:T(1024)}, u32[]{:S(2)}) copy-start(f32[2048]{0:T(1024)} %param.15) | copy-start | bytes 24580
  8.0 172.2 %all-gather.14.cloned.1.call-start = ((), (), s32[]{:S(2)}) async-start(), calls=%async_computation.5 | async-start | bytes 4587520 | tf_op jit(solution)/shard_map/all_gather | solution.py:41
  8.8 243.5 %all-gather.16.cloned.1.call-start = ((), (), s32[]{:S(2)}) async-start(), calls=%async_computation.6 | async-start | bytes 4587520 | tf_op jit(solution)/shard_map/all_gather | solution.py:47
  9.3 282.6 %reduce-scatter.4.cloned.1.call-start = ((), (), s32[]{:S(2)}) async-start(), calls=%async_computation.7 | async-start | bytes 2621440 | tf_op jit(solution)/shard_map/reduce_scatter | solution.py:50
  34.2 73.7 %copy-start.4 = (bf16[512,2048]{1,0:T(8,128)(2,1)S(1)}, bf16[512,2048]{1,0:T(8,128)(2,1)}, u32[]{:S(2)}) copy-start(bf16[512,2048]{1,0:T(8,128)(2,1)} %all-gather.10.cloned.1.call-done) | copy-start | bytes 6291460
  262.0 29.9 %copy-start.2 = (bf16[128,2048]{1,0:T(8,128)(2,1)S(1)}, bf16[128,2048]{1,0:T(8,128)(2,1)}, u32[]{:S(2)}) copy-start(bf16[128,2048]{1,0:T(8,128)(2,1)} %param.14) | copy-start | bytes 1572868
  262.0 54.6 %all-gather.18.cloned.1.call-start = ((), (), s32[]{:S(2)}) async-start(), calls=%async_computation.8 | async-start | bytes 2621440 | tf_op jit(solution)/shard_map/all_gather | solution.py:67
  293.9 70.0 %copy-start.11 = (f32[2048]{0:T(1024)S(1)}, f32[2048]{0:T(1024)}, u32[]{:S(2)}) copy-start(f32[2048]{0:T(1024)} %param.20) | copy-start | bytes 24580
  293.9 70.0 %all-gather.22.cloned.1.call-start = ((), (), s32[]{:S(2)}) async-start(), calls=%async_computation.10 | async-start | bytes 2621440 | tf_op jit(solution)/shard_map/all_gather | solution.py:74
  294.7 115.3 %all-gather.20.cloned.1.call-start = ((), (), s32[]{:S(2)}) async-start(), calls=%async_computation.9 | async-start | bytes 2621440 | tf_op jit(solution)/shard_map/all_gather | solution.py:73
  295.4 160.6 %all-gather.24.cloned.1.call-start = ((), (), s32[]{:S(2)}) async-start(), calls=%async_computation.11 | async-start | bytes 2621440 | tf_op jit(solution)/shard_map/all_gather | solution.py:96
  296.2 196.5 %reduce-scatter.6.cloned.1.call-start = ((), (), s32[]{:S(2)}) async-start(), calls=%async_computation.12 | async-start | bytes 2621440 | tf_op jit(solution)/shard_map/reduce_scatter | solution.py:99
  316.6 47.3 %copy-start.3 = (bf16[512,2048]{1,0:T(8,128)(2,1)S(1)}, bf16[512,2048]{1,0:T(8,128)(2,1)}, u32[]{:S(2)}) copy-start(bf16[512,2048]{1,0:T(8,128)(2,1)} %all-gather.18.cloned.1.call-done) | copy-start | bytes 6291460
  318.9 55.7 %copy-start.7 = (f32[512]{0:T(512)S(1)}, f32[512]{0:T(512)}, u32[]{:S(2)}) copy-start(f32[512]{0:T(512)} %param.24) | copy-start | bytes 6148
  318.9 55.7 %copy-start.8 = (f32[512]{0:T(512)S(1)}, f32[512]{0:T(512)}, u32[]{:S(2)}) copy-start(f32[512]{0:T(512)} %param.23) | copy-start | bytes 6148
  368.0 8.9 %copy-start.6 = (bf16[4,128,128]{2,1,0:T(8,128)(2,1)S(1)}, bf16[4,128,128]{2,1,0:T(8,128)(2,1)}, u32[]{:S(2)}) copy-start(bf16[4,128,128]{2,1,0:T(8,128)(2,1)} %param.25) | copy-start | bytes 393220
  368.0 8.9 %copy-start.9 = (f32[4,128]{1,0:T(4,128)S(1)}, f32[4,128]{1,0:T(4,128)}, u32[]{:S(2)}) copy-start(f32[4,128]{1,0:T(4,128)} %param.26) | copy-start | bytes 6148
  462.5 30.2 %copy-start = (bf16[128,2048]{1,0:T(8,128)(2,1)S(1)}, bf16[128,2048]{1,0:T(8,128)(2,1)}, u32[]{:S(2)}) copy-start(bf16[128,2048]{1,0:T(8,128)(2,1)} %add_convert_fusion.3) | copy-start | bytes 1572868
  462.5 57.1 %copy-start.12 = (f32[2048]{0:T(1024)S(1)}, f32[2048]{0:T(1024)}, u32[]{:S(2)}) copy-start(f32[2048]{0:T(1024)} %param.16) | copy-start | bytes 24580
  462.5 54.8 %all-gather.26.cloned.1.call-start = ((), (), s32[]{:S(2)}) async-start(), calls=%async_computation.13 | async-start | bytes 2621440 | tf_op jit(solution)/shard_map/all_gather | solution.py:20
  494.6 71.7 %reduce-scatter.8.cloned.1.call-start = ((), (), s32[]{:S(2)}) async-start(), calls=%async_computation.14 | async-start | bytes 2621440 | tf_op jit(solution)/shard_map/reduce_scatter | solution.py:50
  517.4 2.2 copy-start.5
  535.0 31.4 %copy-start.1 = (bf16[128,2048]{1,0:T(8,128)(2,1)S(1)}, bf16[128,2048]{1,0:T(8,128)(2,1)}, u32[]{:S(2)}) copy-start(bf16[128,2048]{1,0:T(8,128)(2,1)} %add_convert_fusion.1) | copy-start | bytes 1572868
Sparse Core Ops, SparseCore 0:
  8.9 25.2 all-gather.9
  35.8 72.0 all-gather.11
  109.5 70.6 all-gather.13
  181.6 70.6 all-gather.15
  262.1 29.7 reduce-scatter.3
  294.1 22.5 all-gather.17
  318.2 45.6 all-gather.21
  365.5 44.4 all-gather.19
  411.5 44.4 all-gather.23
  462.6 29.9 reduce-scatter.5
  494.8 22.5 all-gather.25
  535.1 31.1 reduce-scatter.7
where the time goes:
time: 576 us; the launch traced here: 575 us
  waiting for transfers between devices  495 us (86%)
  matrix products  42.7 us (7%)
  other arithmetic  14.1 us (2%)
  between operations  13.7 us (2%)
  blocking collectives  6.51 us (1%)
    all_gather x1, waiting for transfers between devices, half_again(): lax.all_gather(proj_down, 'fs', axis=1, tiled=True)  72.1 us
    all_gather x1, waiting for transfers between devices, half_again(): lax.all_gather(proj_gate, 'fs', axis=0, tiled=True)  71.5 us
    all_gather x1, waiting for transfers between devices, half_again(): lax.all_gather(proj_lift, 'fs', axis=0, tiled=True)  66.6 us
    reduce_scatter x2, waiting for transfers between devices, half_again(): lax.psum_scatter(partial_value.astype(jnp.bfloat16), 'tp', scatter_dimens...  61.2 us
    all_gather x2, waiting for transfers between devices, gathered_norm(): gathered = lax.all_gather(stream_rows, 'tp', axis=0, tiled=True)  47.3 us
    all_gather x1, waiting for transfers between devices, token_mixer(): lax.all_gather(mixer_down, 'fs', axis=1, tiled=True)  46.1 us
    all_gather x1, waiting for transfers between devices, token_mixer(): lax.all_gather(mixer_v, 'fs', axis=0, tiled=True)  45 us
    all_gather x1, waiting for transfers between devices, token_mixer(): lax.all_gather(mixer_u, 'fs', axis=0, tiled=True)  30.2 us
  transfers between devices with their start and end apart: 12, of which 12 were waited for; matrix products, arithmetic and copies ran while one was open for 3% of the time, Pallas kernels for 0%

commit v1 on v0

--- a/solution.py
+++ b/solution.py
@@ -17,7 +17,14 @@
 
 
 def gathered_norm(stream_rows, scale_gain):
-    gathered = lax.all_gather(stream_rows, "tp", axis=0, tiled=True)
+    ways, here = (lax.axis_size("tp"), lax.axis_index("tp"))
+    gathered, reach = (stream_rows, 1)
+    while reach < ways:
+        theirs = lax.ppermute(gathered, "tp", [(d, d ^ reach) for d in range(ways)])
+        mine_first = jnp.concatenate([gathered, theirs], axis=0)
+        theirs_first = jnp.concatenate([theirs, gathered], axis=0)
+        gathered = jnp.where(here & reach == 0, mine_first, theirs_first)
+        reach = 2 * reach
     return norm_rows(gathered, scale_gain)
 
 

time: 576 us -> 552 us (0.958)
  waiting for transfers between devices: 495 us -> 473 us
    ppermute x0 -> x4, waiting for transfers between devices: none -> 51.7 us  [gathered_norm(): theirs = lax.ppermute(gathered, 'tp', [(d, d ^ reach) for d in range(ways)])]
    all_gather x2 -> x0, waiting for transfers between devices: 47.3 us -> none  [gathered_norm(): gathered = lax.all_gather(stream_rows, 'tp', axis=0, tiled=True)]
    all_gather x1, waiting for transfers between devices: 71.5 us -> 45.5 us  [half_again(): lax.all_gather(proj_gate, 'fs', axis=0, tiled=True)]
  transfers between devices with their start and end apart: 12 -> 14, of which waited for: 12 -> 14; matrix products, arithmetic and copies ran while one was open for 3% -> 3% of each run, Pallas kernels for 0% -> 0%
where the time goes in v1:
time: 552 us
  waiting for transfers between devices  473 us (86%)
  matrix products  40.7 us (7%)
  between operations  13.7 us (2%)
  other arithmetic  10.9 us (2%)
  blocking collectives  6.69 us (1%)
    all_gather x1, waiting for transfers between devices, half_again(): lax.all_gather(proj_down, 'fs', axis=1, tiled=True)  72.3 us
    all_gather x1, waiting for transfers between devices, half_again(): lax.all_gather(proj_lift, 'fs', axis=0, tiled=True)  66.6 us
    reduce_scatter x2, waiting for transfers between devices, half_again(): lax.psum_scatter(partial_value.astype(jnp.bfloat16), 'tp', scatter_dimens...  61.2 us
    ppermute x4, waiting for transfers between devices, gathered_norm(): theirs = lax.ppermute(gathered, 'tp', [(d, d ^ reach) for d in range(ways)])  51.7 us
    all_gather x1, waiting for transfers between devices, token_mixer(): lax.all_gather(mixer_down, 'fs', axis=1, tiled=True)  46.1 us
    all_gather x1, waiting for transfers between devices, half_again(): lax.all_gather(proj_gate, 'fs', axis=0, tiled=True)  45.5 us
    all_gather x1, waiting for transfers between devices, token_mixer(): lax.all_gather(mixer_v, 'fs', axis=0, tiled=True)  44.9 us
    all_gather x1, waiting for transfers between devices, token_mixer(): lax.all_gather(mixer_u, 'fs', axis=0, tiled=True)  30.1 us
  transfers between devices with their start and end apart: 14, of which 14 were waited for; matrix products, arithmetic and copies ran while one was open for 3% of the time, Pallas kernels for 0%

profile of v1, /device:TPU:0, one launch (start us, length us, event | category | flops | bytes accessed | tf_op | source)
XLA Modules:
  0.0 551.5 jit_solution(7864095533583845701)
XLA Ops:
  9.4 1.5 collective-permute-done
  11.2 2.9 collective-permute-start.1
  14.1 23.5 %collective-permute-done.1 = bf16[256,2048]{1,0:T(8,128)(2,1)S(1)} collective-permute-done((bf16[256,2048]{1,0:T(8,128)(2,1)S(1)}, bf16[256,2048]{1,0:T(8,128)(2,1)S(1)}, u32[]{:S(2)}, u32[]{:S(2)}) %collective-permute-start.1) | collective-permute-done | bytes 1048608 | tf_op jit(solution)/shard_map/ppermute | solution.py:23
  37.5 0.8 fusion
  38.3 45.5 %all-gather.8.cloned.1.call-done = bf16[2048,896]{1,0:T(8,128)(2,1)} async-done(((bf16[512,896]{1,0:T(8,128)(2,1)}), bf16[2048,896]{1,0:T(8,128)(2,1)}) %all-gather.8.cloned.1.call-update) | async-done | bytes 3670032 | tf_op jit(solution)/shard_map/all_gather | solution.py:47
  83.8 5.7 %fusion.42 = f32[512,896]{1,0:T(8,128)} fusion(bf16[2048,896]{1,0:T(8,128)(2,1)} %all-gather.8.cloned.1.call-done, f32[2048]{0:T(1024)S(1)} %copy-done.8, f32[512]{0:T(512)S(1)} %add_rsqrt_fusion.3, bf16[256,2048]{1,0:T(8,128)(2,1)S(1)} %collective-permute-done.1, bf16[256,2048]{1,0:T(8,128)(2,1)S(1)} %maximum_select_fusion.2, pred[]{:T(512)S(6)} %eq.8), kind=kOutput, calls=%fused_computation.52 | convolution fusion | flops 1892679680 | bytes 7612417 | tf_op jit(solution)/shard_map/dot_general | solution.py:33
  89.4 66.6 %all-gather.10.cloned.1.call-done = bf16[2048,896]{1,0:T(8,128)(2,1)} async-done(((bf16[512,896]{1,0:T(8,128)(2,1)}), bf16[2048,896]{1,0:T(8,128)(2,1)}) %all-gather.10.cloned.1.call-update) | async-done | bytes 3670032 | tf_op jit(solution)/shard_map/all_gather | solution.py:48
  156.0 72.3 %all-gather.12.cloned.1.call-done = bf16[896,2048]{1,0:T(8,128)(2,1)} async-done(((bf16[896,512]{1,0:T(8,128)(2,1)}), bf16[896,2048]{1,0:T(8,128)(2,1)}) %all-gather.12.cloned.1.call-update) | async-done | bytes 3670032 | tf_op jit(solution)/shard_map/all_gather | solution.py:54
  228.3 9.7 %convolution_convert_fusion.1 = bf16[512,2048]{1,0:T(8,128)(2,1)} fusion(bf16[896,2048]{1,0:T(8,128)(2,1)} %all-gather.12.cloned.1.call-done, f32[512,896]{1,0:T(8,128)} %fusion.42, bf16[2048,896]{1,0:T(8,128)(2,1)} %all-gather.10.cloned.1.call-done, f32[2048]{0:T(1024)S(1)} %copy-done.8, f32[512]{0:T(512)S(1)} %add_rsqrt_fusion.3, ...), kind=kOutput, calls=%fused_computation.16 | convolution fusion | flops 3775528960 | bytes 13379585 | tf_op jit(solution)/shard_map/dot_general | solution.py:52
  238.0 29.9 %reduce-scatter.4.cloned.1.call-done = bf16[128,2048]{1,0:T(8,128)(2,1)} async-done(((bf16[512,2048]{1,0:T(8,128)(2,1)}), bf16[128,2048]{1,0:T(8,128)(2,1)}) %reduce-scatter.4.cloned.1.call-update) | async-done | bytes 524304 | tf_op jit(solution)/shard_map/reduce_scatter | solution.py:57
  267.9 2.0 add_convert_fusion.3
  272.1 20.6 %all-gather.14.cloned.1.call-done = bf16[512,2048]{1,0:T(8,128)(2,1)} async-done(((bf16[128,2048]{1,0:T(8,128)(2,1)}), bf16[512,2048]{1,0:T(8,128)(2,1)}) %all-gather.14.cloned.1.call-update) | async-done | bytes 2097168 | tf_op jit(solution)/shard_map/all_gather | solution.py:74
  292.6 2.2 fusion.3
  294.9 44.9 %all-gather.18.cloned.1.call-done = bf16[2048,512]{1,0:T(8,128)(2,1)} async-done(((bf16[512,512]{1,0:T(8,128)(2,1)}), bf16[2048,512]{1,0:T(8,128)(2,1)}) %all-gather.18.cloned.1.call-update) | async-done | bytes 2097168 | tf_op jit(solution)/shard_map/all_gather | solution.py:81
  339.8 4.1 fusion.60
  343.9 6.7 %all-reduce = (f32[512]{0:T(512)S(1)}, f32[512]{0:T(512)S(1)}) all-reduce(f32[512]{0:T(512)S(1)} %get-tuple-element.6, f32[512]{0:T(512)S(1)} %get-tuple-element.5), channel_id=1, replica_groups=mesh['rep'=2,'fs'=4,'tp'=4] {'tp'}, use_global_device_ids=true, to_apply=%region_6.7 | all-reduce | flops 1024 | bytes 8192 | tf_op jit(solution)/shard_map/psum | solution.py:85
  350.6 1.5 add_convert_fusion.2
  352.1 0.9 reshape.47
  353.0 1.4 fusion.9
  354.4 1.3 copy.21
  355.7 30.1 %all-gather.16.cloned.1.call-done = bf16[2048,512]{1,0:T(8,128)(2,1)} async-done(((bf16[512,512]{1,0:T(8,128)(2,1)}), bf16[2048,512]{1,0:T(8,128)(2,1)}) %all-gather.16.cloned.1.call-update) | async-done | bytes 2097168 | tf_op jit(solution)/shard_map/all_gather | solution.py:80
  385.8 46.1 %all-gather.20.cloned.1.call-done = bf16[512,2048]{1,0:T(8,128)(2,1)} async-done(((bf16[512,512]{1,0:T(8,128)(2,1)}), bf16[512,2048]{1,0:T(8,128)(2,1)}) %all-gather.20.cloned.1.call-update) | async-done | bytes 2097168 | tf_op jit(solution)/shard_map/all_gather | solution.py:103
  431.9 6.5 %convolution_convert_fusion.2 = bf16[512,2048]{1,0:T(8,128)(2,1)} fusion(bf16[512,2048]{1,0:T(8,128)(2,1)} %all-gather.20.cloned.1.call-done, f32[64,8,4,128]{3,2,1,0:T(4,128)} %bitcast.25, bf16[2048,512]{1,0:T(8,128)(2,1)} %all-gather.16.cloned.1.call-done, bf16[512,2048]{1,0:T(8,128)(2,1)S(1)} %copy-done.2, f32[2048]{0:T(1024)S(1)} %copy-done.9, ...), kind=kOutput, calls=%fused_computation.17 | convolution fusion | flops 2155347968 | bytes 9447424 | tf_op jit(solution)/shard_map/dot_general | solution.py:101
  438.4 30.1 %reduce-scatter.6.cloned.1.call-done = bf16[128,2048]{1,0:T(8,128)(2,1)} async-done(((bf16[512,2048]{1,0:T(8,128)(2,1)}), bf16[128,2048]{1,0:T(8,128)(2,1)}) %reduce-scatter.6.cloned.1.call-update) | async-done | bytes 524304 | tf_op jit(solution)/shard_map/reduce_scatter | solution.py:106
  468.5 1.2 add_convert_fusion.1
  469.8 1.9 collective-permute-done.2
  472.4 24.9 %collective-permute-done.3 = bf16[256,2048]{1,0:T(8,128)(2,1)S(1)} collective-permute-done((bf16[256,2048]{1,0:T(8,128)(2,1)S(1)}, bf16[256,2048]{1,0:T(8,128)(2,1)S(1)}, u32[]{:S(2)}, u32[]{:S(2)}) %collective-permute-start.3) | collective-permute-done | bytes 1048608 | tf_op jit(solution)/shard_map/ppermute | solution.py:23
  497.2 0.8 fusion.6
  498.0 3.6 fusion.28
  501.6 9.7 %convolution_convert_fusion = bf16[512,2048]{1,0:T(8,128)(2,1)} fusion(bf16[896,2048]{1,0:T(8,128)(2,1)} %all-gather.12.cloned.1.call-done, f32[512,896]{1,0:T(8,128)} %fusion.28, bf16[2048,896]{1,0:T(8,128)(2,1)} %all-gather.10.cloned.1.call-done, f32[2048]{0:T(1024)S(1)} %copy-done.10, f32[512]{0:T(512)S(1)} %add_rsqrt_fusion, ...), kind=kOutput, calls=%fused_computation.15 | convolution fusion | flops 3775528960 | bytes 13379585 | tf_op jit(solution)/shard_map/dot_general | solution.py:52
  511.3 31.3 %reduce-scatter.8.cloned.1.call-done = bf16[128,2048]{1,0:T(8,128)(2,1)} async-done(((bf16[512,2048]{1,0:T(8,128)(2,1)}), bf16[128,2048]{1,0:T(8,128)(2,1)}) %reduce-scatter.8.cloned.1.call-update) | async-done | bytes 524304 | tf_op jit(solution)/shard_map/reduce_scatter | solution.py:57
  542.7 2.0 add_convert_fusion
  (52 shorter events, 6.1 us)
Async XLA Ops:
  6.5 2.3 copy-start.1
  6.5 77.2 %all-gather.8.cloned.1.call-start = ((), (), s32[]{:S(2)}) async-start(), calls=%async_computation.3 | async-start | bytes 4587520 | tf_op jit(solution)/shard_map/all_gather | solution.py:47
  7.3 148.8 %all-gather.10.cloned.1.call-start = ((), (), s32[]{:S(2)}) async-start(), calls=%async_computation.4 | async-start | bytes 4587520 | tf_op jit(solution)/shard_map/all_gather | solution.py:48
  8.0 220.3 %all-gather.12.cloned.1.call-start = ((), (), s32[]{:S(2)}) async-start(), calls=%async_computation.5 | async-start | bytes 4587520 | tf_op jit(solution)/shard_map/all_gather | solution.py:54
  8.7 259.2 %reduce-scatter.4.cloned.1.call-start = ((), (), s32[]{:S(2)}) async-start(), calls=%async_computation.6 | async-start | bytes 2621440 | tf_op jit(solution)/shard_map/reduce_scatter | solution.py:57
  8.8 2.1 collective-permute-start
  9.4 74.4 %copy-start.8 = (f32[2048]{0:T(1024)S(1)}, f32[2048]{0:T(1024)}, u32[]{:S(2)}) copy-start(f32[2048]{0:T(1024)} %param.15) | copy-start | bytes 24580
  11.2 26.4 %collective-permute-start.1 = (bf16[256,2048]{1,0:T(8,128)(2,1)S(1)}, bf16[256,2048]{1,0:T(8,128)(2,1)S(1)}, u32[]{:S(2)}, u32[]{:S(2)}) collective-permute-start(bf16[256,2048]{1,0:T(8,128)(2,1)S(1)} %maximum_select_fusion.2), channel_id=1, source_target_pairs={{0,2},{1,3},{2,0},{3,1},{4,6},{5,7},{6,4},{7,5},{8,10},{9,11},{10,... | collective-permute-start | bytes 3145736 | tf_op jit(solution)/shard_map/ppermute | solution.py:23
  238.0 54.6 %all-gather.14.cloned.1.call-start = ((), (), s32[]{:S(2)}) async-start(), calls=%async_computation.7 | async-start | bytes 2621440 | tf_op jit(solution)/shard_map/all_gather | solution.py:74
  269.9 69.9 %copy-start.9 = (f32[2048]{0:T(1024)S(1)}, f32[2048]{0:T(1024)}, u32[]{:S(2)}) copy-start(f32[2048]{0:T(1024)} %param.20) | copy-start | bytes 24580
  269.9 69.8 %all-gather.18.cloned.1.call-start = ((), (), s32[]{:S(2)}) async-start(), calls=%async_computation.9 | async-start | bytes 2621440 | tf_op jit(solution)/shard_map/all_gather | solution.py:81
  270.5 115.3 %all-gather.16.cloned.1.call-start = ((), (), s32[]{:S(2)}) async-start(), calls=%async_computation.8 | async-start | bytes 2621440 | tf_op jit(solution)/shard_map/all_gather | solution.py:80
  271.3 160.6 %all-gather.20.cloned.1.call-start = ((), (), s32[]{:S(2)}) async-start(), calls=%async_computation.10 | async-start | bytes 2621440 | tf_op jit(solution)/shard_map/all_gather | solution.py:103
  272.0 196.5 %reduce-scatter.6.cloned.1.call-start = ((), (), s32[]{:S(2)}) async-start(), calls=%async_computation.11 | async-start | bytes 2621440 | tf_op jit(solution)/shard_map/reduce_scatter | solution.py:106
  292.6 47.1 %copy-start.2 = (bf16[512,2048]{1,0:T(8,128)(2,1)S(1)}, bf16[512,2048]{1,0:T(8,128)(2,1)}, u32[]{:S(2)}) copy-start(bf16[512,2048]{1,0:T(8,128)(2,1)} %all-gather.14.cloned.1.call-done) | copy-start | bytes 6291460
  294.9 55.7 %copy-start.4 = (f32[512]{0:T(512)S(1)}, f32[512]{0:T(512)}, u32[]{:S(2)}) copy-start(f32[512]{0:T(512)} %param.24) | copy-start | bytes 6148
  294.9 55.7 %copy-start.5 = (f32[512]{0:T(512)S(1)}, f32[512]{0:T(512)}, u32[]{:S(2)}) copy-start(f32[512]{0:T(512)} %param.23) | copy-start | bytes 6148
  343.9 9.1 %copy-start.3 = (bf16[4,128,128]{2,1,0:T(8,128)(2,1)S(1)}, bf16[4,128,128]{2,1,0:T(8,128)(2,1)}, u32[]{:S(2)}) copy-start(bf16[4,128,128]{2,1,0:T(8,128)(2,1)} %param.25) | copy-start | bytes 393220
  343.9 9.1 %copy-start.6 = (f32[4,128]{1,0:T(4,128)S(1)}, f32[4,128]{1,0:T(4,128)}, u32[]{:S(2)}) copy-start(f32[4,128]{1,0:T(4,128)} %param.26) | copy-start | bytes 6148
  438.4 30.2 %copy-start = (bf16[128,2048]{1,0:T(8,128)(2,1)S(1)}, bf16[128,2048]{1,0:T(8,128)(2,1)}, u32[]{:S(2)}) copy-start(bf16[128,2048]{1,0:T(8,128)(2,1)} %add_convert_fusion.3) | copy-start | bytes 1572868
  438.4 104.3 %reduce-scatter.8.cloned.1.call-start = ((), (), s32[]{:S(2)}) async-start(), calls=%async_computation.12 | async-start | bytes 2621440 | tf_op jit(solution)/shard_map/reduce_scatter | solution.py:57
  469.7 28.3 %copy-start.7 = (bf16[2048,896]{1,0:T(8,128)(2,1)S(1)}, bf16[2048,896]{1,0:T(8,128)(2,1)}, u32[]{:S(2)}) copy-start(bf16[2048,896]{1,0:T(8,128)(2,1)} %all-gather.8.cloned.1.call-done) | copy-start | bytes 11010052
  469.7 28.3 %copy-start.10 = (f32[2048]{0:T(1024)S(1)}, f32[2048]{0:T(1024)}, u32[]{:S(2)}) copy-start(f32[2048]{0:T(1024)} %param.16) | copy-start | bytes 24580
  469.7 2.0 collective-permute-start.2
  471.9 25.3 %collective-permute-start.3 = (bf16[256,2048]{1,0:T(8,128)(2,1)S(1)}, bf16[256,2048]{1,0:T(8,128)(2,1)S(1)}, u32[]{:S(2)}, u32[]{:S(2)}) collective-permute-start(bf16[256,2048]{1,0:T(8,128)(2,1)S(1)} %maximum_select_fusion.3), channel_id=1, source_target_pairs={{0,2},{1,3},{2,0},{3,1},{4,6},{5,7},{6,4},{7,5},{8,10},{9,11},{10,... | collective-permute-start | bytes 3145736 | tf_op jit(solution)/shard_map/ppermute | solution.py:23
Sparse Core Ops, SparseCore 0:
  8.9 74.8 all-gather.7
  85.3 70.6 all-gather.9
  157.6 70.6 all-gather.11
  238.1 29.7 reduce-scatter.3
  270.0 22.5 all-gather.13
  294.1 45.6 all-gather.17
  341.3 44.4 all-gather.15
  387.4 44.4 all-gather.19
  438.5 29.9 reduce-scatter.5
  511.5 31.1 reduce-scatter.7
